TPU v7x, 256 devices: a whole 4x4x8 slice. The times are simulated.
256 devices in a mesh: sp: 64 (over z, x, core), tp: 4 (over y).
Axes of the slice: x: 4, y: 4, z: 8, core: 2. Of those that a mesh axis runs over, the one named last changes fastest.
Arguments:
- residual_in: bfloat16 [16384, 2048], P('sp', 'tp'), may hold values from -6 to 6
- conv_input: bfloat16 [16384, 512], P('sp', 'tp'), may hold values from -6 to 6
- outer_gate: bfloat16 [16384, 512], P('sp', 'tp'), may hold values from -6 to 6
- inner_gate: bfloat16 [16384, 512], P('sp', 'tp'), may hold values from -6 to 6
- documents: int32 [16384], P('sp'), may hold values from 0 to 31, as said below
- conv_taps: float32 [3, 512], P(None, 'tp'), may hold values from -3 to 3
- mixer_gain: float32 [512], replicated, may hold values from 0.1 to 1.9
- output_weight: bfloat16 [512, 2048], P(None, 'tp'), may hold values from -0.25 to 0.25
- ffn_gain: float32 [2048], P('tp'), may hold values from 0.1 to 1.9
- routes: int32 [16384, 2], P('sp'), may hold values from 0 to 63, all different within a row; in each aligned block of 256 rows (0 to 255, 256 to 511, ...) at most 16 rows name the same one
- route_weights: float32 [16384, 2], P('sp'), may hold values from 0.1 to 0.9
- expert_gate: bfloat16 [64, 2048, 3584], P('sp', None, 'tp'), may hold values from -0.125 to 0.125
- expert_up: bfloat16 [64, 2048, 3584], P('sp', None, 'tp'), may hold values from -0.125 to 0.125
- expert_down: bfloat16 [64, 3584, 2048], P('sp', 'tp'), may hold values from -0.09375 to 0.09375
Outputs:
- layer_out: bfloat16 [16384, 2048], P('sp', 'tp')
Inputs may be any that keep to these rules, and one draw needn't show every extreme that they name: Document numbers never fall along the positions, and each of the 32 documents occurs. Every document has 256 to 768 positions, and one has exactly 768. `routes`: the two experts of a position differ. Among the 256 positions of one index of sp no expert is named more than 16 times, a bound that some block reaches.
All inputs are finite; a program needn't handle non-finite values.
Results may differ from a plain program's by a relative error of at most 0.0058.
Values may be sent and summed in bfloat16 or wider, within the bound.
A program may use at most 64 MiB of HBM per device.

v0:
```python
import jax
import jax.numpy as jnp
from jax import lax
from jax.sharding import PartitionSpec as P

EPS = 1e-06


def from_behind(block, axis, distance):
    devices = range(lax.axis_size(axis))
    route = [(i - distance, i) for i in devices if i - distance in devices]
    return lax.ppermute(block, axis, route)


def laid_out(pieces, dim):
    dims = list(pieces.shape[1:])
    dims[dim] *= pieces.shape[0]
    return jnp.moveaxis(pieces, 0, dim).reshape(dims)


def sent_to_all(shard, axis):
    copies = jnp.broadcast_to(shard, (lax.axis_size(axis), *shard.shape))
    return lax.all_to_all(copies, axis, split_axis=0, concat_axis=0, tiled=True)


def gather_directly(shard, axis, dim):
    return laid_out(sent_to_all(shard, axis), dim)


def over_copies(shard, axis):
    return sent_to_all(shard, axis).sum(axis=0)


def slot_tables(routes, experts, capacity):
    tokens = routes.shape[0]
    flattened = routes.reshape(-1)
    onehot = (flattened[:, None] == jnp.arange(experts, dtype=jnp.int32)[None, :]).astype(jnp.int32)
    earlier = jnp.cumsum(onehot, axis=0) - onehot
    position_in = jnp.sum(earlier * onehot, axis=1)
    target = flattened * capacity + position_in
    owners = (
        jnp.full((experts * capacity,), tokens, jnp.int32)
        .at[target]
        .set(jnp.arange(2 * tokens, dtype=jnp.int32) // 2)
    )
    return (target, owners)


def per_device(
    residual_in,
    conv_input,
    outer_gate,
    inner_gate,
    documents,
    conv_taps,
    mixer_gain,
    output_weight,
    ffn_gain,
    routes,
    route_weights,
    expert_gate,
    expert_up,
    expert_down,
):
    tokens_here = residual_in.shape[0]
    local_features = residual_in.shape[1]
    conv_value = (inner_gate.astype(jnp.float32) * conv_input.astype(jnp.float32)).astype(
        jnp.bfloat16
    )
    doc_marks = documents.astype(jnp.bfloat16)
    before_rows, before_docs = from_behind((conv_value[-2:], doc_marks[-2:]), "sp", 1)
    joined_rows = jnp.concatenate([before_rows, conv_value], axis=0).astype(jnp.float32)
    joined_docs = jnp.concatenate([before_docs, doc_marks], axis=0)
    same_one = (joined_docs[1:-1] == doc_marks).astype(jnp.float32)[:, None]
    same_two = (joined_docs[:-2] == doc_marks).astype(jnp.float32)[:, None]
    conv_sum = (
        conv_taps[2] * joined_rows[2:]
        + conv_taps[1] * joined_rows[1:-1] * same_one
        + conv_taps[0] * joined_rows[:-2] * same_two
    )
    mixed = (outer_gate.astype(jnp.float32) * conv_sum).astype(jnp.bfloat16)
    piece_f = gather_directly(mixed, "tp", 1).astype(jnp.float32)
    scaled = (piece_f * mixer_gain).astype(jnp.bfloat16)
    accum = jnp.dot(scaled, output_weight, preferred_element_type=jnp.float32)
    squares = jnp.sum(piece_f * piece_f, axis=1)
    mix_scale = lax.rsqrt(squares / mixer_gain.shape[0] + EPS)
    hidden_state = residual_in.astype(jnp.float32) + accum * mix_scale[:, None]
    feature_total = over_copies(jnp.sum(hidden_state * hidden_state, axis=1), "tp")
    model_width = local_features * lax.axis_size("tp")
    normed = (
        hidden_state * lax.rsqrt(feature_total / model_width + EPS)[:, None] * ffn_gain
    ).astype(jnp.bfloat16)
    experts = lax.axis_size("sp") * expert_gate.shape[0]
    capacity = 4 * tokens_here // experts
    target, owners = slot_tables(routes, experts, capacity)
    padded = jnp.concatenate([normed, jnp.zeros((1, local_features), jnp.bfloat16)], axis=0)
    outgoing = padded[owners].reshape(experts, capacity, local_features)
    slices_in = lax.all_to_all(outgoing, "sp", split_axis=0, concat_axis=0, tiled=True)
    arrived = lax.all_gather(slices_in, "tp", axis=2, tiled=True)
    expert_in = arrived.reshape(-1, model_width)
    gate = jnp.dot(expert_in, expert_gate[0], preferred_element_type=jnp.float32)
    upper = jnp.dot(expert_in, expert_up[0], preferred_element_type=jnp.float32)
    act = (jax.nn.silu(gate) * upper).astype(jnp.bfloat16)
    partial_out = jnp.dot(act, expert_down[0], preferred_element_type=jnp.float32)
    summed = lax.psum_scatter(
        partial_out.astype(jnp.bfloat16), "tp", scatter_dimension=1, tiled=True
    )
    returned = lax.all_to_all(
        summed.reshape(experts, capacity, local_features),
        "sp",
        split_axis=0,
        concat_axis=0,
        tiled=True,
    )
    picked = returned.reshape(experts * capacity, local_features)[target].astype(jnp.float32)
    picked = picked.reshape(tokens_here, 2, local_features)
    routed = jnp.sum(picked * route_weights[:, :, None], axis=1)
    return (hidden_state + routed).astype(jnp.bfloat16)


def solution(mesh):
    placed = (
        P("sp", "tp"),
        P("sp", "tp"),
        P("sp", "tp"),
        P("sp", "tp"),
        P("sp"),
        P(None, "tp"),
        P(),
        P(None, "tp"),
        P("tp"),
        P("sp", None),
        P("sp", None),
        P("sp", None, "tp"),
        P("sp", None, "tp"),
        P("sp", "tp", None),
    )
    return jax.shard_map(
        per_device, mesh=mesh, in_specs=placed, out_specs=P("sp", "tp"), check_vma=False
    )
```

profile of v0, /device:TPU:1, one launch (start us, length us, event | category | flops | bytes accessed | tf_op | source)
XLA Modules:
  0.0 252.4 jit_solution(10328017283454354348)
XLA Ops:
  6.5 0.8 convert_element_type.78
  7.3 0.1 slice.41
  7.4 4.5 %collective-permute-start.1 = (bf16[2]{0:T(256)(128)(2,1)S(1)}, bf16[2]{0:T(256)(128)(2,1)S(1)}, u32[]{:S(2)}, u32[]{:S(2)}) collective-permute-start(bf16[2]{0:T(256)(128)(2,1)S(1)} %slice.41), channel_id=1, source_target_pairs={{0,4},{4,8},{8,12},{12,16},{16,20},{20,24},{24,28},{28,32},{32,36}... | collective-permute-start | bytes 20 | tf_op jit(solution)/shard_map/ppermute | solution.py:12
  11.9 0.9 multiply_convert_fusion.2
  12.8 1.9 collective-permute-start
  14.7 0.8 copy.31
  15.5 0.1 eq.37
  15.7 0.1 eq.33
  15.8 0.7 broadcast_multiply_fusion
  16.5 0.8 slice_bitcast_fusion.2
  17.3 1.2 reduce-window.6
  18.5 0.2 slice_reduce_fusion
  18.8 0.1 copy.30
  18.9 0.1 mul.153
  19.1 0.1 fusion.11
  19.2 0.1 pad_maximum_fusion
  19.3 0.8 compare_convert_fusion.1
  20.1 1.0 fusion.15
  21.1 0.1 copy.28
  21.2 0.7 broadcast_in_dim.8
  21.9 4.2 %all-to-all-start = ((bf16[4,256,128]{1,2,0:T(8,128)(2,1)}), bf16[4,256,128]{1,2,0:T(8,128)(2,1)S(1)}, u32[]{:S(2)}, u32[]{:S(2)}) async-start(bf16[4,256,128]{1,2,0:T(8,128)(2,1)} %broadcast_in_dim.8), calls=%async_computation | async-start | bytes 524288 | tf_op jit(solution)/shard_map/all_to_all | solution.py:23
  26.1 2.4 scatter_custom_fusion
  28.5 3.2 %all-to-all-done = bf16[4,256,128]{1,2,0:T(8,128)(2,1)S(1)} async-done(((bf16[4,256,128]{1,2,0:T(8,128)(2,1)}), bf16[4,256,128]{1,2,0:T(8,128)(2,1)S(1)}, u32[]{:S(2)}, u32[]{:S(2)}) %all-to-all-start) | async-done | bytes 262176 | tf_op jit(solution)/shard_map/all_to_all | solution.py:23
  31.8 0.1 multiply_reduce_fusion.2
  31.9 0.8 fusion.8
  32.7 0.4 multiply_reduce_fusion.1
  33.2 0.6 broadcast_in_dim.9
  33.8 3.2 %all-to-all-start.1 = ((f32[4,1,256]{2,1,0:T(1,128)}), f32[4,1,256]{2,1,0:T(1,128)S(1)}, u32[]{:S(2)}, u32[]{:S(2)}) async-start(f32[4,1,256]{2,1,0:T(1,128)} %broadcast_in_dim.9), calls=%async_computation.1 | async-start | bytes 8192 | tf_op jit(solution)/shard_map/all_to_all | solution.py:23
  37.0 0.0 all-gather.2.cloned.1.call-start
  37.1 4.0 %all-to-all-done.1 = f32[4,1,256]{2,1,0:T(1,128)S(1)} async-done(((f32[4,1,256]{2,1,0:T(1,128)}), f32[4,1,256]{2,1,0:T(1,128)S(1)}, u32[]{:S(2)}, u32[]{:S(2)}) %all-to-all-start.1) | async-done | bytes 4128 | tf_op jit(solution)/shard_map/all_to_all | solution.py:23
  41.2 0.1 multiply_convert_fusion.1
  41.3 4.0 %gather_fusion = bf16[1024,512]{1,0:T(8,128)(2,1)S(1)} fusion(bf16[257,512]{1,0:T(8,128)(2,1)S(1)} %concatenate.11, s32[1024]{0:T(1024)S(1)} %fusion.19), kind=kCustom, calls=%fused_computation | custom fusion | bytes 2101248 | tf_op jit(solution)/shard_map/gather | solution.py:97
  45.3 42.3 %all_to_all.21 = bf16[64,16,512]{2,1,0:T(8,128)(2,1)} all-to-all(bf16[64,16,512]{2,1,0:T(8,128)(2,1)S(1)} %bitcast.54), channel_id=1, replica_groups=mesh['sp'=64,'tp'=4] {'sp'}, dimensions={0} | all-to-all | bytes 2097152 | tf_op jit(solution)/shard_map/all_to_all | solution.py:98
  87.6 0.0 all-gather.2.cloned.1.call-update
  87.7 0.0 reduce-scatter.2.cloned.1.call-start
  87.7 45.8 %all-gather.2.cloned.1.call-done = bf16[64,16,2048]{2,1,0:T(8,128)(2,1)} async-done(((bf16[64,16,512]{2,1,0:T(8,128)(2,1)}), bf16[64,16,2048]{2,1,0:T(8,128)(2,1)}) %all-gather.2.cloned.1.call-update) | async-done | bytes 4194320 | tf_op jit(solution)/shard_map/all_gather | solution.py:99
  133.5 7.5 %fusion.1 = f32[1024,896]{1,0:T(8,128)S(1)} fusion(bf16[1024,2048]{1,0:T(8,128)(2,1)} %bitcast.59, bf16[1,2048,896]{2,1,0:T(8,128)(2,1)} %param.26), kind=kOutput, calls=%fused_computation.5 | convolution fusion | flops 3758096384 | bytes 11534336 | tf_op jit(solution)/shard_map/dot_general | solution.py:102
  141.0 4.8 %multiply_convert_fusion = bf16[1024,896]{1,0:T(8,128)(2,1)S(1)} fusion(f32[1024,896]{1,0:T(8,128)S(1)} %fusion.1, bf16[1024,2048]{1,0:T(8,128)(2,1)S(1)} %bitcast.60, bf16[1,2048,896]{2,1,0:T(8,128)(2,1)S(1)} %copy-done.5), kind=kOutput, calls=%fused_computation.9 | convolution fusion | flops 3763601408 | bytes 13369344 | tf_op jit(solution)/shard_map/dot_general | solution.py:101
  145.9 6.1 %convolution_convert_fusion = bf16[1024,2048]{1,0:T(8,128)(2,1)} fusion(bf16[1024,896]{1,0:T(8,128)(2,1)S(1)} %multiply_convert_fusion, bf16[1,896,2048]{2,1,0:T(8,128)(2,1)S(1)} %copy-done.6), kind=kOutput, calls=%fused_computation.3 | convolution fusion | flops 3760193536 | bytes 9699328 | tf_op jit(solution)/shard_map/dot_general | solution.py:104
  151.9 0.0 reduce-scatter.2.cloned.1.call-update
  151.9 50.0 %reduce-scatter.2.cloned.1.call-done = bf16[1024,512]{1,0:T(8,128)(2,1)} async-done(((bf16[1024,2048]{1,0:T(8,128)(2,1)}), bf16[1024,512]{1,0:T(8,128)(2,1)}) %reduce-scatter.2.cloned.1.call-update) | async-done | bytes 1048592 | tf_op jit(solution)/shard_map/reduce_scatter | solution.py:105
  202.0 10.7 %all-to-all-start.3 = ((bf16[64,16,512]{2,1,0:T(8,128)(2,1)}), bf16[64,16,512]{2,1,0:T(8,128)(2,1)S(1)}, u32[]{:S(2)}, u32[]{:S(2)}) async-start(bf16[64,16,512]{2,1,0:T(8,128)(2,1)} %bitcast.55), calls=%async_computation.4 | async-start | bytes 2097152 | tf_op jit(solution)/shard_map/all_to_all | solution.py:108
  212.7 0.1 copy.34
  212.8 28.0 %all-to-all-done.3 = bf16[64,16,512]{2,1,0:T(8,128)(2,1)S(1)} async-done(((bf16[64,16,512]{2,1,0:T(8,128)(2,1)}), bf16[64,16,512]{2,1,0:T(8,128)(2,1)S(1)}, u32[]{:S(2)}, u32[]{:S(2)}) %all-to-all-start.3) | async-done | bytes 1048608 | tf_op jit(solution)/shard_map/all_to_all | solution.py:108
  240.8 2.0 gather_fusion.1
  242.8 0.7 reshape.90
  243.5 1.3 multiply_reduce_fusion
  244.8 0.8 add_convert_fusion
  (29 shorter events, 0.2 us)
Async XLA Ops:
  6.5 26.2 %copy-start = (bf16[512,512]{1,0:T(8,128)(2,1)S(1)}, bf16[512,512]{1,0:T(8,128)(2,1)}, u32[]{:S(2)}) copy-start(bf16[512,512]{1,0:T(8,128)(2,1)} %param.21) | copy-start | bytes 1572868
  6.5 26.2 %copy-start.1 = (bf16[256,512]{1,0:T(8,128)(2,1)S(1)}, bf16[256,512]{1,0:T(8,128)(2,1)}, u32[]{:S(2)}) copy-start(bf16[256,512]{1,0:T(8,128)(2,1)} %param.14) | copy-start | bytes 786436
  6.5 34.6 %copy-start.2 = (f32[512]{0:T(512)S(1)}, f32[512]{0:T(512)}, u32[]{:S(2)}) copy-start(f32[512]{0:T(512)} %param.22) | copy-start | bytes 6148
  7.4 11.8 %collective-permute-start.1 = (bf16[2]{0:T(256)(128)(2,1)S(1)}, bf16[2]{0:T(256)(128)(2,1)S(1)}, u32[]{:S(2)}, u32[]{:S(2)}) collective-permute-start(bf16[2]{0:T(256)(128)(2,1)S(1)} %slice.41), channel_id=1, source_target_pairs={{0,4},{4,8},{8,12},{12,16},{16,20},{20,24},{24,28},{28,32},{32,36}... | collective-permute-start | bytes 20 | tf_op jit(solution)/shard_map/ppermute | solution.py:12
  12.8 7.3 %collective-permute-start = (bf16[2,128]{1,0:T(2,128)(2,1)S(1)}, bf16[2,128]{1,0:T(2,128)(2,1)S(1)}, u32[]{:S(2)}, u32[]{:S(2)}) collective-permute-start(bf16[2,128]{1,0:T(2,128)(2,1)S(1)} %slice.52), channel_id=1, source_target_pairs={{0,4},{4,8},{8,12},{12,16},{16,20},{20,24},{24,28},{28,32},{32,36}... | collective-permute-start | bytes 1544 | tf_op jit(solution)/shard_map/ppermute | solution.py:12
  21.9 9.9 %all-to-all-start = ((bf16[4,256,128]{1,2,0:T(8,128)(2,1)}), bf16[4,256,128]{1,2,0:T(8,128)(2,1)S(1)}, u32[]{:S(2)}, u32[]{:S(2)}) async-start(bf16[4,256,128]{1,2,0:T(8,128)(2,1)} %broadcast_in_dim.8), calls=%async_computation | async-start | bytes 524288 | tf_op jit(solution)/shard_map/all_to_all | solution.py:23
  33.8 7.4 %all-to-all-start.1 = ((f32[4,1,256]{2,1,0:T(1,128)}), f32[4,1,256]{2,1,0:T(1,128)S(1)}, u32[]{:S(2)}, u32[]{:S(2)}) async-start(f32[4,1,256]{2,1,0:T(1,128)} %broadcast_in_dim.9), calls=%async_computation.1 | async-start | bytes 8192 | tf_op jit(solution)/shard_map/all_to_all | solution.py:23
  37.0 96.5 %all-gather.2.cloned.1.call-start = ((), (), s32[]{:S(2)}) async-start(), calls=%async_computation.5 | async-start | bytes 5242880 | tf_op jit(solution)/shard_map/all_gather | solution.py:99
  87.7 114.3 %reduce-scatter.2.cloned.1.call-start = ((), (), s32[]{:S(2)}) async-start(), calls=%async_computation.6 | async-start | bytes 5242880 | tf_op jit(solution)/shard_map/reduce_scatter | solution.py:105
  133.5 7.5 %copy-start.4 = (bf16[64,16,2048]{2,1,0:T(8,128)(2,1)S(1)}, bf16[64,16,2048]{2,1,0:T(8,128)(2,1)}, u32[]{:S(2)}) copy-start(bf16[64,16,2048]{2,1,0:T(8,128)(2,1)} %all-gather.2.cloned.1.call-done) | copy-start | bytes 12582916
  133.5 7.5 %copy-start.5 = (bf16[1,2048,896]{2,1,0:T(8,128)(2,1)S(1)}, bf16[1,2048,896]{2,1,0:T(8,128)(2,1)}, u32[]{:S(2)}) copy-start(bf16[1,2048,896]{2,1,0:T(8,128)(2,1)} %param.25) | copy-start | bytes 11010052
  141.0 4.8 %copy-start.6 = (bf16[1,896,2048]{2,1,0:T(8,128)(2,1)S(1)}, bf16[1,896,2048]{2,1,0:T(8,128)(2,1)}, u32[]{:S(2)}) copy-start(bf16[1,896,2048]{2,1,0:T(8,128)(2,1)} %param.27) | copy-start | bytes 11010052
  151.9 60.8 %copy-start.3 = (f32[256,2]{0,1:T(2,128)S(1)}, f32[256,2]{0,1:T(2,128)}, u32[]{:S(2)}) copy-start(f32[256,2]{0,1:T(2,128)} %param.24) | copy-start | bytes 6148
  202.0 38.9 %all-to-all-start.3 = ((bf16[64,16,512]{2,1,0:T(8,128)(2,1)}), bf16[64,16,512]{2,1,0:T(8,128)(2,1)S(1)}, u32[]{:S(2)}, u32[]{:S(2)}) async-start(bf16[64,16,512]{2,1,0:T(8,128)(2,1)} %bitcast.55), calls=%async_computation.4 | async-start | bytes 2097152 | tf_op jit(solution)/shard_map/all_to_all | solution.py:108
Sparse Core Ops, SparseCore 0:
  87.8 45.6 all-gather.1
  152.1 49.8 reduce-scatter.1
where the time goes:
time: 253 us; the launch traced here: 252 us
  waiting for transfers between devices  131 us (52%)
  blocking collectives  42.3 us (17%)
  starting transfers between devices  24.6 us (10%)
  matrix products  18.8 us (7%)
  between operations  13.7 us (5%)
  local copies, waits for them, and re-layouts  13.1 us (5%)
  other arithmetic  8.73 us (3%)
    reduce_scatter x1, waiting for transfers between devices, per_device(): lax.psum_scatter(partial_out.astype(jnp.bfloat16), 'tp', scatter_dimensio...  50 us
    all_gather x1, waiting for transfers between devices, per_device(): arrived = lax.all_gather(slices_in, 'tp', axis=2, tiled=True)  45.8 us
    all_to_all x1, blocking collectives, per_device(): lax.all_to_all(outgoing, 'sp', split_axis=0, concat_axis=0, tiled=True)  42.3 us
    all_to_all x1, waiting for transfers between devices, per_device(): lax.all_to_all(summed.reshape(experts, capacity, local_features), 'sp', s...  28 us
    all_to_all x1, starting transfers between devices, per_device(): lax.all_to_all(summed.reshape(experts, capacity, local_features), 'sp', s...  10.7 us
    dot_general x1, matrix products, per_device(): upper = jnp.dot(expert_in, expert_up[0], preferred_element_type=jnp.float32)  7.49 us
    all_to_all x2, starting transfers between devices, sent_to_all(): return lax.all_to_all(copies, axis, split_axis=0, concat_axis=0, tiled=True)  7.43 us
    all_to_all x2, waiting for transfers between devices, sent_to_all(): return lax.all_to_all(copies, axis, split_axis=0, concat_axis=0, tiled=True)  7.29 us
  transfers between devices with their start and end apart: 7, of which 5 were waited for; matrix products, arithmetic and copies ran while one was open for 3% of the time, Pallas kernels for 0%

commit v1 on v0

--- a/solution.py
+++ b/solution.py
@@ -4,6 +4,12 @@
 from jax.sharding import PartitionSpec as P
 
 EPS = 1e-06
+
+
+def laid_out_2(blocks, dim):
+    shape = list(blocks.shape[1:])
+    shape[dim] *= blocks.shape[0]
+    return jnp.moveaxis(blocks, 0, dim).reshape(shape)
 
 
 def from_behind(block, axis, distance):
@@ -96,7 +102,19 @@
     padded = jnp.concatenate([normed, jnp.zeros((1, local_features), jnp.bfloat16)], axis=0)
     outgoing = padded[owners].reshape(experts, capacity, local_features)
     slices_in = lax.all_to_all(outgoing, "sp", split_axis=0, concat_axis=0, tiled=True)
-    arrived = lax.all_gather(slices_in, "tp", axis=2, tiled=True)
+    size = lax.axis_size("tp")
+    pairs = [(i_2, (i_2 + 1) % size) for i_2 in range(size)]
+    back = [(b, a) for a, b in pairs]
+    lower, upper_2 = ([], [])
+    for step in range(size - 1):
+        if step % 2 == 0:
+            lower.append(lax.ppermute(lower[-1] if lower else slices_in, "tp", pairs))
+        else:
+            upper_2.append(lax.ppermute(upper_2[-1] if upper_2 else slices_in, "tp", back))
+    tiles = jnp.stack([*lower[::-1], slices_in, *upper_2])
+    shift = lax.axis_index("tp") - len(lower)
+    tiles = tiles[(jnp.arange(size) - shift) % size]
+    arrived = laid_out_2(tiles, 2)
     expert_in = arrived.reshape(-1, model_width)
     gate = jnp.dot(expert_in, expert_gate[0], preferred_element_type=jnp.float32)
     upper = jnp.dot(expert_in, expert_up[0], preferred_element_type=jnp.float32)

time: 253 us -> 271 us (1.071)
  local copies, waits for them, and re-layouts: 13.1 us -> 30.6 us
  other arithmetic: 8.73 us -> 12.2 us
  waiting for transfers between devices: 131 us -> 128 us
  matrix products: 18.8 us -> 16 us
    ppermute x0 -> x3, waiting for transfers between devices: none -> 46.1 us  [the longest x2 46.1 us: per_device(): lower.append(lax.ppermute(lower[-1] if lower else slices_in, 'tp', pairs))]
    all_gather x1 -> x0, waiting for transfers between devices: 45.8 us -> none  [per_device(): arrived = lax.all_gather(slices_in, 'tp', axis=2, tiled=True)]
    transpose x0 -> x1, local copies, waits for them, and re-layouts: none -> 10.5 us  [laid_out_2(): return jnp.moveaxis(blocks, 0, dim).reshape(shape)]
    gather x0 -> x1, local copies, waits for them, and re-layouts: none -> 4.97 us  [per_device(): tiles = tiles[(jnp.arange(size) - shift) % size]]
    another operation x2 -> x3, other arithmetic: 1.24 us -> 4.66 us  [the longest x1 3.42 us: per_device(): tiles = jnp.stack([*lower[::-1], slices_in, *upper_2])]
    reduce_scatter x1, waiting for transfers between devices: 50 us -> 46.7 us  [per_device(): lax.psum_scatter(partial_out.astype(jnp.bfloat16), 'tp', scatter_dimensio...]
    dot_general x1, matrix products: 7.49 us -> 4.73 us  [per_device(): upper = jnp.dot(expert_in, expert_up[0], preferred_element_type=jnp.float32)]
  transfers between devices with their start and end apart: 7 -> 9, of which waited for: 5 -> 6; matrix products, arithmetic and copies ran while one was open for 3% -> 3% of each run, Pallas kernels for 0% -> 0%
where the time goes in v1:
time: 271 us; the launch traced here: 270 us
  waiting for transfers between devices  128 us (47%)
  blocking collectives  42.2 us (16%)
  local copies, waits for them, and re-layouts  30.6 us (11%)
  starting transfers between devices  27.3 us (10%)
  matrix products  16 us (6%)
  between operations  13.7 us (5%)
  other arithmetic  12.2 us (5%)
    reduce_scatter x1, waiting for transfers between devices, per_device(): lax.psum_scatter(partial_out.astype(jnp.bfloat16), 'tp', scatter_dimensio...  46.7 us
    ppermute x2, waiting for transfers between devices, per_device(): lower.append(lax.ppermute(lower[-1] if lower else slices_in, 'tp', pairs))  46.1 us
    all_to_all x1, blocking collectives, per_device(): lax.all_to_all(outgoing, 'sp', split_axis=0, concat_axis=0, tiled=True)  42.2 us
    all_to_all x1, waiting for transfers between devices, per_device(): lax.all_to_all(summed.reshape(experts, capacity, local_features), 'sp', s...  28 us
    all_to_all x1, starting transfers between devices, per_device(): lax.all_to_all(summed.reshape(experts, capacity, local_features), 'sp', s...  10.7 us
    transpose x1, local copies, waits for them, and re-layouts, laid_out_2(): return jnp.moveaxis(blocks, 0, dim).reshape(shape)  10.5 us
    all_to_all x2, starting transfers between devices, sent_to_all(): return lax.all_to_all(copies, axis, split_axis=0, concat_axis=0, tiled=True)  7.43 us
    all_to_all x2, waiting for transfers between devices, sent_to_all(): return lax.all_to_all(copies, axis, split_axis=0, concat_axis=0, tiled=True)  7.29 us
  transfers between devices with their start and end apart: 9, of which 6 were waited for; matrix products, arithmetic and copies ran while one was open for 3% of the time, Pallas kernels for 0%

profile of v1, /device:TPU:1, one launch (start us, length us, event | category | flops | bytes accessed | tf_op | source)
XLA Modules:
  0.0 270.1 jit_solution(891647064858020380)
XLA Ops:
  6.5 0.8 convert_element_type.78
  7.4 4.5 %collective-permute-start.1 = (bf16[2]{0:T(256)(128)(2,1)S(1)}, bf16[2]{0:T(256)(128)(2,1)S(1)}, u32[]{:S(2)}, u32[]{:S(2)}) collective-permute-start(bf16[2]{0:T(256)(128)(2,1)S(1)} %slice.41), channel_id=1, source_target_pairs={{0,4},{4,8},{8,12},{12,16},{16,20},{20,24},{24,28},{28,32},{32,36}... | collective-permute-start | bytes 20 | tf_op jit(solution)/shard_map/ppermute | solution.py:18
  11.9 0.9 multiply_convert_fusion.2
  12.8 1.9 collective-permute-start
  14.7 0.8 copy.39
  15.5 0.1 eq.39
  15.7 0.1 eq.35
  15.8 0.7 broadcast_multiply_fusion
  16.5 0.8 slice_bitcast_fusion.2
  17.3 1.2 reduce-window.6
  18.5 0.2 slice_reduce_fusion
  18.8 0.1 copy.38
  18.9 0.1 mul.153
  19.1 0.1 fusion.11
  19.3 0.8 compare_convert_fusion.1
  20.1 1.0 fusion.15
  21.2 0.7 broadcast_in_dim.8
  21.9 4.2 %all-to-all-start = ((bf16[4,256,128]{1,2,0:T(8,128)(2,1)}), bf16[4,256,128]{1,2,0:T(8,128)(2,1)S(1)}, u32[]{:S(2)}, u32[]{:S(2)}) async-start(bf16[4,256,128]{1,2,0:T(8,128)(2,1)} %broadcast_in_dim.8), calls=%async_computation | async-start | bytes 524288 | tf_op jit(solution)/shard_map/all_to_all | solution.py:29
  26.1 2.4 scatter_custom_fusion
  28.5 3.2 %all-to-all-done = bf16[4,256,128]{1,2,0:T(8,128)(2,1)S(1)} async-done(((bf16[4,256,128]{1,2,0:T(8,128)(2,1)}), bf16[4,256,128]{1,2,0:T(8,128)(2,1)S(1)}, u32[]{:S(2)}, u32[]{:S(2)}) %all-to-all-start) | async-done | bytes 262176 | tf_op jit(solution)/shard_map/all_to_all | solution.py:29
  31.9 0.8 fusion.8
  32.7 0.4 multiply_reduce_fusion.1
  33.2 0.6 broadcast_in_dim.9
  33.8 3.2 %all-to-all-start.1 = ((f32[4,1,256]{2,1,0:T(1,128)}), f32[4,1,256]{2,1,0:T(1,128)S(1)}, u32[]{:S(2)}, u32[]{:S(2)}) async-start(f32[4,1,256]{2,1,0:T(1,128)} %broadcast_in_dim.9), calls=%async_computation.1 | async-start | bytes 8192 | tf_op jit(solution)/shard_map/all_to_all | solution.py:29
  37.1 4.0 %all-to-all-done.1 = f32[4,1,256]{2,1,0:T(1,128)S(1)} async-done(((f32[4,1,256]{2,1,0:T(1,128)}), f32[4,1,256]{2,1,0:T(1,128)S(1)}, u32[]{:S(2)}, u32[]{:S(2)}) %all-to-all-start.1) | async-done | bytes 4128 | tf_op jit(solution)/shard_map/all_to_all | solution.py:29
  41.2 0.1 multiply_convert_fusion.1
  41.3 4.0 %gather_fusion = bf16[1024,512]{1,0:T(8,128)(2,1)S(1)} fusion(bf16[257,512]{1,0:T(8,128)(2,1)S(1)} %concatenate.11, s32[1024]{0:T(1024)S(1)} %fusion.19), kind=kCustom, calls=%fused_computation | custom fusion | bytes 2101248 | tf_op jit(solution)/shard_map/gather | solution.py:103
  45.3 42.2 %all_to_all.21 = bf16[64,16,512]{2,1,0:T(8,128)(2,1)S(1)} all-to-all(bf16[64,16,512]{2,1,0:T(8,128)(2,1)S(1)} %bitcast.65), channel_id=1, replica_groups=mesh['sp'=64,'tp'=4] {'sp'}, dimensions={0} | all-to-all | bytes 2097152 | tf_op jit(solution)/shard_map/all_to_all | solution.py:104
  87.5 0.3 collective-permute-start.2
  87.8 2.4 collective-permute-start.4
  90.2 22.1 %collective-permute-done.2 = bf16[64,16,512]{2,1,0:T(8,128)(2,1)S(1)} collective-permute-done((bf16[64,16,512]{2,1,0:T(8,128)(2,1)S(1)}, bf16[64,16,512]{2,1,0:T(8,128)(2,1)S(1)}, u32[]{:S(2)}, u32[]{:S(2)}) %collective-permute-start.2) | collective-permute-done | bytes 1048608 | tf_op jit(solution)/shard_map/ppermute | solution.py:111
  112.3 24.0 %collective-permute-done.3 = bf16[64,16,512]{2,1,0:T(8,128)(2,1)} collective-permute-done((bf16[64,16,512]{2,1,0:T(8,128)(2,1)S(1)}, bf16[64,16,512]{2,1,0:T(8,128)(2,1)}, u32[]{:S(2)}, u32[]{:S(2)}) %collective-permute-start.3) | collective-permute-done | bytes 1048608 | tf_op jit(solution)/shard_map/ppermute | solution.py:111
  136.3 3.4 %pad_maximum_fusion = bf16[4,64,16,512]{3,2,1,0:T(8,128)(2,1)} fusion(bf16[1,64,16,512]{3,2,1,0:T(8,128)(2,1)} %bitcast.12, bf16[1,64,16,512]{3,2,1,0:T(8,128)(2,1)S(1)} %bitcast.68, bf16[1,64,16,512]{3,2,1,0:T(8,128)(2,1)S(1)} %bitcast.70, bf16[1,64,16,512]{3,2,1,0:T(8,128)(2,1)} %bitcast.9), kind=kLoop, calls=%fused_computation.4 | loop fusion | flops 6291456 | bytes 8388608 | tf_op jit(solution)/shard_map/stack | solution.py:114
  139.7 5.0 %gather_fusion.1 = bf16[4,64,16,512]{3,2,1,0:T(8,128)(2,1)} fusion(bf16[4,64,16,512]{3,2,1,0:T(8,128)(2,1)} %pad_maximum_fusion, s32[1024]{0:T(1024)S(1)} %pad_clamp_fusion.1), kind=kCustom, calls=%fused_computation.1 | custom fusion | bytes 8388624 | tf_op jit(solution)/shard_map/gather | solution.py:116
  144.7 10.5 %copy.42 = bf16[64,16,4,512]{3,2,1,0:T(4,128)(2,1)S(1)} copy(bf16[64,16,4,512]{3,1,0,2:T(8,128)(2,1)} %bitcast.63) | data formatting | bytes 8388608 | tf_op jit(solution)/shard_map/transpose | solution.py:12
  155.2 1.4 copy.46
  156.7 0.6 copy-done.4
  157.3 4.7 %fusion.1 = f32[1024,896]{1,0:T(8,128)S(1)} fusion(bf16[1024,2048]{1,0:T(8,128)(2,1)S(1)} %bitcast.66, bf16[1,2048,896]{2,1,0:T(8,128)(2,1)S(1)} %copy-done.4), kind=kOutput, calls=%fused_computation.7 | convolution fusion | flops 3758096384 | bytes 11534336 | tf_op jit(solution)/shard_map/dot_general | solution.py:120
  162.0 4.8 %multiply_convert_fusion = bf16[1024,896]{1,0:T(8,128)(2,1)S(1)} fusion(f32[1024,896]{1,0:T(8,128)S(1)} %fusion.1, bf16[1024,2048]{1,0:T(8,128)(2,1)S(1)} %bitcast.67, bf16[1,2048,896]{2,1,0:T(8,128)(2,1)S(1)} %copy-done.5), kind=kOutput, calls=%fused_computation.11 | convolution fusion | flops 3763601408 | bytes 13369344 | tf_op jit(solution)/shard_map/dot_general | solution.py:119
  166.9 6.1 %convolution_convert_fusion = bf16[1024,2048]{1,0:T(8,128)(2,1)} fusion(bf16[1024,896]{1,0:T(8,128)(2,1)S(1)} %multiply_convert_fusion, bf16[1,896,2048]{2,1,0:T(8,128)(2,1)S(1)} %copy-done.6), kind=kOutput, calls=%fused_computation.5 | convolution fusion | flops 3760193536 | bytes 9699328 | tf_op jit(solution)/shard_map/dot_general | solution.py:122
  173.0 46.7 %reduce-scatter.2.cloned.1.call-done = bf16[1024,512]{1,0:T(8,128)(2,1)} async-done(((bf16[1024,2048]{1,0:T(8,128)(2,1)}), bf16[1024,512]{1,0:T(8,128)(2,1)}) %reduce-scatter.2.cloned.1.call-update) | async-done | bytes 1048592 | tf_op jit(solution)/shard_map/reduce_scatter | solution.py:123
  219.7 10.7 %all-to-all-start.3 = ((bf16[64,16,512]{2,1,0:T(8,128)(2,1)}), bf16[64,16,512]{2,1,0:T(8,128)(2,1)S(1)}, u32[]{:S(2)}, u32[]{:S(2)}) async-start(bf16[64,16,512]{2,1,0:T(8,128)(2,1)} %bitcast.69), calls=%async_computation.4 | async-start | bytes 2097152 | tf_op jit(solution)/shard_map/all_to_all | solution.py:126
  230.4 0.1 copy.43
  230.6 28.0 %all-to-all-done.3 = bf16[64,16,512]{2,1,0:T(8,128)(2,1)S(1)} async-done(((bf16[64,16,512]{2,1,0:T(8,128)(2,1)}), bf16[64,16,512]{2,1,0:T(8,128)(2,1)S(1)}, u32[]{:S(2)}, u32[]{:S(2)}) %all-to-all-start.3) | async-done | bytes 1048608 | tf_op jit(solution)/shard_map/all_to_all | solution.py:126
  258.6 2.0 gather_fusion.2
  260.5 0.7 reshape.135
  261.2 1.3 multiply_reduce_fusion
  262.5 0.8 add_convert_fusion
  (38 shorter events, 0.6 us)
Async XLA Ops:
  6.5 26.2 %copy-start = (bf16[512,512]{1,0:T(8,128)(2,1)S(1)}, bf16[512,512]{1,0:T(8,128)(2,1)}, u32[]{:S(2)}) copy-start(bf16[512,512]{1,0:T(8,128)(2,1)} %param.21) | copy-start | bytes 1572868
  6.5 26.2 %copy-start.1 = (bf16[256,512]{1,0:T(8,128)(2,1)S(1)}, bf16[256,512]{1,0:T(8,128)(2,1)}, u32[]{:S(2)}) copy-start(bf16[256,512]{1,0:T(8,128)(2,1)} %param.14) | copy-start | bytes 786436
  6.5 34.6 %copy-start.2 = (f32[512]{0:T(512)S(1)}, f32[512]{0:T(512)}, u32[]{:S(2)}) copy-start(f32[512]{0:T(512)} %param.22) | copy-start | bytes 6148
  7.4 11.8 %collective-permute-start.1 = (bf16[2]{0:T(256)(128)(2,1)S(1)}, bf16[2]{0:T(256)(128)(2,1)S(1)}, u32[]{:S(2)}, u32[]{:S(2)}) collective-permute-start(bf16[2]{0:T(256)(128)(2,1)S(1)} %slice.41), channel_id=1, source_target_pairs={{0,4},{4,8},{8,12},{12,16},{16,20},{20,24},{24,28},{28,32},{32,36}... | collective-permute-start | bytes 20 | tf_op jit(solution)/shard_map/ppermute | solution.py:18
  12.8 7.3 %collective-permute-start = (bf16[2,128]{1,0:T(2,128)(2,1)S(1)}, bf16[2,128]{1,0:T(2,128)(2,1)S(1)}, u32[]{:S(2)}, u32[]{:S(2)}) collective-permute-start(bf16[2,128]{1,0:T(2,128)(2,1)S(1)} %slice.54), channel_id=1, source_target_pairs={{0,4},{4,8},{8,12},{12,16},{16,20},{20,24},{24,28},{28,32},{32,36}... | collective-permute-start | bytes 1544 | tf_op jit(solution)/shard_map/ppermute | solution.py:18
  21.9 9.9 %all-to-all-start = ((bf16[4,256,128]{1,2,0:T(8,128)(2,1)}), bf16[4,256,128]{1,2,0:T(8,128)(2,1)S(1)}, u32[]{:S(2)}, u32[]{:S(2)}) async-start(bf16[4,256,128]{1,2,0:T(8,128)(2,1)} %broadcast_in_dim.8), calls=%async_computation | async-start | bytes 524288 | tf_op jit(solution)/shard_map/all_to_all | solution.py:29
  33.8 7.4 %all-to-all-start.1 = ((f32[4,1,256]{2,1,0:T(1,128)}), f32[4,1,256]{2,1,0:T(1,128)S(1)}, u32[]{:S(2)}, u32[]{:S(2)}) async-start(f32[4,1,256]{2,1,0:T(1,128)} %broadcast_in_dim.9), calls=%async_computation.1 | async-start | bytes 8192 | tf_op jit(solution)/shard_map/all_to_all | solution.py:29
  37.0 182.6 %reduce-scatter.2.cloned.1.call-start = ((), (), s32[]{:S(2)}) async-start(), calls=%async_computation.5 | async-start | bytes 5242880 | tf_op jit(solution)/shard_map/reduce_scatter | solution.py:123
  87.5 24.8 %collective-permute-start.2 = (bf16[64,16,512]{2,1,0:T(8,128)(2,1)S(1)}, bf16[64,16,512]{2,1,0:T(8,128)(2,1)S(1)}, u32[]{:S(2)}, u32[]{:S(2)}) collective-permute-start(bf16[64,16,512]{2,1,0:T(8,128)(2,1)S(1)} %all_to_all.21), channel_id=1, source_target_pairs={{0,1},{1,2},{2,3},{3,0},{4,5},{5,6},{6,7},{7,4},{8,9},{9,10},{10,1... | collective-permute-start | bytes 3145736 | tf_op jit(solution)/shard_map/ppermute | solution.py:111
  87.8 24.5 %collective-permute-start.4 = (bf16[64,16,512]{2,1,0:T(8,128)(2,1)S(1)}, bf16[64,16,512]{2,1,0:T(8,128)(2,1)}, u32[]{:S(2)}, u32[]{:S(2)}) collective-permute-start(bf16[64,16,512]{2,1,0:T(8,128)(2,1)S(1)} %all_to_all.21), channel_id=1, source_target_pairs={{1,0},{2,1},{3,2},{0,3},{5,4},{6,5},{7,6},{4,7},{9,8},{10,9},{11,1... | collective-permute-start | bytes 3145736 | tf_op jit(solution)/shard_map/ppermute | solution.py:113
  112.3 24.0 %collective-permute-start.3 = (bf16[64,16,512]{2,1,0:T(8,128)(2,1)S(1)}, bf16[64,16,512]{2,1,0:T(8,128)(2,1)}, u32[]{:S(2)}, u32[]{:S(2)}) collective-permute-start(bf16[64,16,512]{2,1,0:T(8,128)(2,1)S(1)} %collective-permute-done.2), channel_id=1, source_target_pairs={{0,1},{1,2},{2,3},{3,0},{4,5},{5,6},{6,7},{7,4},{8,9},{9,10},{10,1... | collective-permute-start | bytes 3145736 | tf_op jit(solution)/shard_map/ppermute | solution.py:111
  155.2 2.0 copy-start.4
  157.3 4.7 %copy-start.5 = (bf16[1,2048,896]{2,1,0:T(8,128)(2,1)S(1)}, bf16[1,2048,896]{2,1,0:T(8,128)(2,1)}, u32[]{:S(2)}) copy-start(bf16[1,2048,896]{2,1,0:T(8,128)(2,1)} %param.25) | copy-start | bytes 11010052
  162.0 4.8 %copy-start.6 = (bf16[1,896,2048]{2,1,0:T(8,128)(2,1)S(1)}, bf16[1,896,2048]{2,1,0:T(8,128)(2,1)}, u32[]{:S(2)}) copy-start(bf16[1,896,2048]{2,1,0:T(8,128)(2,1)} %param.27) | copy-start | bytes 11010052
  172.9 57.5 %copy-start.3 = (f32[256,2]{0,1:T(2,128)S(1)}, f32[256,2]{0,1:T(2,128)}, u32[]{:S(2)}) copy-start(f32[256,2]{0,1:T(2,128)} %param.24) | copy-start | bytes 6148
  219.7 38.9 %all-to-all-start.3 = ((bf16[64,16,512]{2,1,0:T(8,128)(2,1)}), bf16[64,16,512]{2,1,0:T(8,128)(2,1)S(1)}, u32[]{:S(2)}, u32[]{:S(2)}) async-start(bf16[64,16,512]{2,1,0:T(8,128)(2,1)} %bitcast.69), calls=%async_computation.4 | async-start | bytes 2097152 | tf_op jit(solution)/shard_map/all_to_all | solution.py:126
Sparse Core Ops, SparseCore 0:
  173.1 46.5 reduce-scatter.1
